TPU v7x, 512 devices: a whole 4x4x16 slice. The times are simulated.
512 devices in a mesh: sp: 16 (over z), fs: 4 (over y), tp: 8 (over x, core).
Axes of the slice: x: 4, y: 4, z: 16, core: 2. Of those that a mesh axis runs over, the one named last changes fastest.
Arguments:
- tokens: bfloat16 [4, 4096, 2048], P('fs', 'sp'), may hold values from -6 to 6
- mix_gain: float32 [2048], replicated, may hold values from 0.1 to 1.9
- query_down: bfloat16 [2048, 768], P('fs', 'tp'), may hold values from -0.125 to 0.125
- memory_down: bfloat16 [2048, 512], P('fs', 'tp'), may hold values from -0.125 to 0.125
- rope_weight: bfloat16 [2048, 32], replicated, may hold values from -0.125 to 0.125
- query_up: bfloat16 [768, 1536], P('fs', 'tp'), may hold values from -0.21875 to 0.21875
- key_up: bfloat16 [512, 1024], P('fs', 'tp'), may hold values from -0.25 to 0.25
- value_up: bfloat16 [512, 1024], P('fs', 'tp'), may hold values from -0.25 to 0.25
- latent_gain: float32 [768], replicated, may hold values from 0.1 to 1.9
- memory_gain: float32 [512], replicated, may hold values from 0.1 to 1.9
- query_gain: float32 [96], replicated, may hold values from 1 to 16
- key_gain: float32 [96], replicated, may hold values from 0.1 to 1.9
- conv_value: bfloat16 [2048, 1024], P('fs', 'tp'), may hold values from -1 to 1
- conv_gate: bfloat16 [2048, 1024], P('fs', 'tp'), may hold values from -0.125 to 0.125
- conv_kernel: bfloat16 [31, 1024], P(None, 'tp'), may hold values from -50 to 50
- channel_gain: float32 [1024], P('tp'), may hold values from 0.1 to 1.9
- channel_shift: float32 [1024], P('tp'), may hold values from -3 to 3
- heads_out: bfloat16 [1024, 2048], P('tp', 'fs'), may hold values from -0.75 to 0.75
- conv_out: bfloat16 [1024, 2048], P('tp', 'fs'), may hold values from -0.1875 to 0.1875
Outputs:
- mixed: bfloat16 [4, 4096, 2048], P('fs', 'sp')
All inputs are finite; a program needn't handle non-finite values.
Results may differ from a plain program's by a relative error of at most 0.015.
The roundings to bfloat16 on the way count: a program that leaves them out, or rounds other values in their place, can miss the bound.
Values may be sent and summed in bfloat16 or wider, within the bound.
No kernel may reach another device: no remote copies, remote signals or barrier semaphores. Data moves between devices by JAX's collectives and lax.ppermute only.
A program may use at most 64 MiB of HBM per device.

v0:
```python
import jax
import jax.numpy as jnp
from jax import lax
from jax.sharding import PartitionSpec as P

QK_NOPE = 64
QK_ROPE = 32
V_DIM = 64
CONV_W = 1024
SEG = 64
QK_DIM = 96


epsilon = 1e-06
rope_base = 10000.0
masked_score = -1e30


def side_by_side(arrays, axis, dim, along):
    ends, at = ([], 0)
    for a in arrays[:-1]:
        at += a.shape[along]
        ends.append(at)
    both = jnp.concatenate(arrays, axis=along)
    return tuple(jnp.split(lax.all_gather(both, axis, axis=dim, tiled=True), ends, axis=along))


def laid_out(pieces, dim):
    shape = list(pieces.shape[1:])
    shape[dim] *= pieces.shape[0]
    return jnp.moveaxis(pieces, 0, dim).reshape(shape)


def one_gather(arrays, axis, dims):
    vector = jnp.concatenate([a.reshape(-1) for a in arrays])
    lines, at, outs = (lax.all_gather(vector, axis), 0, [])
    for a, dim in zip(arrays, dims):
        pieces = lines[:, at : at + a.size].reshape(-1, *a.shape)
        outs.append(laid_out(pieces, dim))
        at += a.size
    return tuple(outs)


def from_behind(value, axis, by):
    count = lax.axis_size(axis)
    pairs = [(i, i + by) for i in range(count) if 0 <= i + by < count]
    return lax.ppermute(value, axis, pairs)


def sent_to_all(value, axis):
    copies = jnp.broadcast_to(value, (lax.axis_size(axis), *value.shape))
    return lax.all_to_all(copies, axis, split_axis=0, concat_axis=0, tiled=True)


def over_copies(value, axis):
    everything = sent_to_all(value, axis)
    return jnp.sum(everything, axis=0)


def packed_total(arrays, axis):
    vector, at, outs = (jnp.concatenate([a.reshape(-1) for a in arrays]), 0, [])
    total = over_copies(vector, axis)
    for a in arrays:
        outs.append(total[at : at + a.size].reshape(a.shape))
        at += a.size
    return tuple(outs)


def over_pieces(value, axis):
    return lax.all_gather(value, axis).astype(jnp.float32).sum(0)


def norm_rows(matrix, scale_vector):
    return (
        matrix
        * lax.rsqrt(jnp.mean(matrix * matrix, axis=-1, keepdims=True) + epsilon)
        * scale_vector
    )


def rope_tables(positions):
    inverse_freq = 1.0 / rope_base ** (jnp.arange(0, QK_ROPE, 2, dtype=jnp.float32) / QK_ROPE)
    angles = positions.astype(jnp.float32)[:, None] * inverse_freq[None, :]
    return (jnp.cos(angles)[:, None, :], jnp.sin(angles)[:, None, :])


def rotate(matrix, cosine_table, sine_table):
    half_width = matrix.shape[-1] // 2
    front_half = matrix[..., :half_width]
    back_half = matrix[..., half_width:]
    return jnp.concatenate(
        [
            front_half * cosine_table - back_half * sine_table,
            front_half * sine_table + back_half * cosine_table,
        ],
        axis=-1,
    )


def heads_query(latent, weight, scale_vector, cosine_table, sine_table):
    row_count = latent.shape[0]
    projected = jnp.dot(latent, weight, preferred_element_type=jnp.float32)
    projected = norm_rows(
        projected.reshape(row_count, weight.shape[1] // QK_DIM, QK_DIM), scale_vector
    )
    turned = rotate(projected[..., QK_NOPE:], cosine_table, sine_table)
    return jnp.concatenate([projected[..., :QK_NOPE], turned], axis=-1).astype(jnp.bfloat16)


def heads_key(latent, rope_rows, weight, scale_vector, cosine_table, sine_table):
    row_count = latent.shape[0]
    head_count = weight.shape[1] // QK_NOPE
    nope_part = jnp.dot(latent, weight, preferred_element_type=jnp.float32).reshape(
        row_count, head_count, QK_NOPE
    )
    shared = jnp.broadcast_to(
        rope_rows.astype(jnp.float32)[:, None, :], (row_count, head_count, QK_ROPE)
    )
    joined = norm_rows(jnp.concatenate([nope_part, shared], axis=-1), scale_vector)
    turned = rotate(joined[..., QK_NOPE:], cosine_table, sine_table)
    return jnp.concatenate([joined[..., :QK_NOPE], turned], axis=-1).astype(jnp.bfloat16)


def depthwise(extended, kernel, row_count):

    def add_tap(tap_index, running):
        window = lax.dynamic_slice_in_dim(extended, tap_index, row_count, 0).astype(jnp.float32)
        weight_row = lax.dynamic_slice_in_dim(kernel, tap_index, 1, 0).astype(jnp.float32)
        return running + window * weight_row

    return lax.fori_loop(
        0, kernel.shape[0], add_tap, jnp.zeros((row_count, kernel.shape[1]), jnp.float32)
    )


def key_block(key_count):
    block_size = key_count
    while block_size > 2048 and block_size % 2 == 0:
        block_size = block_size // 2
    return block_size


def local(
    tokens,
    mix_gain,
    query_down,
    memory_down,
    rope_weight,
    query_up,
    key_up,
    value_up,
    latent_gain,
    memory_gain,
    query_gain,
    key_gain,
    conv_value,
    conv_gate,
    conv_kernel,
    channel_gain,
    channel_shift,
    heads_out,
    conv_out,
):
    own_rows = tokens[0]
    normed = norm_rows(own_rows.astype(jnp.float32), mix_gain).astype(jnp.bfloat16)
    down_query, down_memory, conv_values, conv_gates, up_query, up_keys, up_values = (
        *side_by_side((query_down, memory_down, conv_value, conv_gate), "fs", 0, 1),
        lax.all_gather(query_up, "fs", axis=0, tiled=True),
        *side_by_side((key_up, value_up), "fs", 0, 1),
    )
    out_heads, out_conv = side_by_side((heads_out, conv_out), "fs", 1, 0)
    joined = jnp.concatenate(
        [down_query, down_memory, rope_weight, conv_values, conv_gates], axis=1
    )
    query_cols = down_query.shape[1]
    memory_cols = down_memory.shape[1]
    conv_cols = conv_values.shape[1]
    projected = jnp.dot(normed, joined, preferred_element_type=jnp.float32)
    row_count = projected.shape[0]
    rope_start = query_cols + memory_cols
    value_start = rope_start + QK_ROPE
    latent_query = projected[:, :query_cols].astype(jnp.bfloat16)
    latent_memory = projected[:, query_cols:rope_start].astype(jnp.bfloat16)
    rope_rows = projected[:, rope_start:value_start].astype(jnp.bfloat16)
    gated = (
        projected[:, value_start : value_start + conv_cols]
        * jax.nn.sigmoid(projected[:, value_start + conv_cols :])
    ).astype(jnp.bfloat16)
    whole_query, whole_memory = one_gather((latent_query, latent_memory), "tp", (1, 1))
    query_normed = norm_rows(whole_query.astype(jnp.float32), latent_gain).astype(jnp.bfloat16)
    memory_normed = norm_rows(whole_memory.astype(jnp.float32), memory_gain).astype(jnp.bfloat16)
    positions = lax.axis_index("sp") * row_count + jnp.arange(row_count, dtype=jnp.int32)
    cosine_table, sine_table = rope_tables(positions)
    queries = heads_query(query_normed, up_query, query_gain, cosine_table, sine_table)
    head_count = queries.shape[1]
    query_segment = positions // SEG
    score_scale = QK_DIM ** (-0.5)
    tap_count = conv_kernel.shape[0]
    left_rim = from_behind(gated[row_count - (tap_count - 1) :], "sp", 1)
    conv_sum = depthwise(jnp.concatenate([left_rim, gated], axis=0), conv_kernel, row_count)
    row_sums, row_squares = packed_total(
        (jnp.sum(conv_sum, axis=1), jnp.sum(conv_sum * conv_sum, axis=1)), "tp"
    )
    row_mean = row_sums / CONV_W
    spread = row_squares / CONV_W - row_mean * row_mean
    centered = conv_sum - row_mean[:, None]
    conv_result = jax.nn.silu(
        centered * lax.rsqrt(spread[:, None] + epsilon) * channel_gain + channel_shift
    ).astype(jnp.bfloat16)

    def attend(state_carry, key_rows, value_rows, key_pos):
        running_max, row_total, weighted = state_carry
        scores = (
            jnp.einsum("qhd,khd->qhk", queries, key_rows, preferred_element_type=jnp.float32)
            * score_scale
        )
        allowed = ((key_pos // SEG)[None, :] <= query_segment[:, None])[:, None, :]
        scores = jnp.where(allowed, scores, masked_score)
        new_max = jnp.maximum(running_max, jnp.max(scores, axis=2))
        weights = jnp.where(allowed, jnp.exp(scores - new_max[:, :, None]), 0.0)
        factor = jnp.exp(running_max - new_max)
        row_total = row_total * factor + jnp.sum(weights, axis=2)
        weighted = weighted * factor[:, :, None] + jnp.einsum(
            "qhk,khd->qhd",
            weights.astype(jnp.bfloat16),
            value_rows,
            preferred_element_type=jnp.float32,
        )
        return (new_max, row_total, weighted)

    initial = (
        jnp.full((row_count, head_count), masked_score, jnp.float32),
        jnp.zeros((row_count, head_count), jnp.float32),
        jnp.zeros((row_count, head_count, V_DIM), jnp.float32),
    )
    own_keys = heads_key(
        memory_normed, rope_rows, up_keys, key_gain, cosine_table, sine_table
    ).reshape(row_count, head_count * QK_DIM)
    own_values = jnp.dot(memory_normed, up_values, preferred_element_type=jnp.float32).astype(
        jnp.bfloat16
    )
    key_piece, value_piece = side_by_side((own_keys, own_values), "sp", 0, 1)

    def block_keys(block_start, block_size):
        key_rows = lax.dynamic_slice_in_dim(key_piece, block_start, block_size, 0).reshape(
            block_size, head_count, QK_DIM
        )
        value_rows = lax.dynamic_slice_in_dim(value_piece, block_start, block_size, 0).reshape(
            block_size, head_count, V_DIM
        )
        key_pos = block_start + jnp.arange(block_size, dtype=jnp.int32)
        return (key_rows, value_rows, key_pos)

    key_count = key_piece.shape[0]
    block_size = key_block(key_count)

    def step(block_index, running):
        key_rows, value_rows, key_pos = block_keys(block_index * block_size, block_size)
        return attend(running, key_rows, value_rows, key_pos)

    final_state = lax.fori_loop(0, key_count // block_size, step, initial)
    running_max, row_total, weighted = final_state
    attention = (
        (weighted / row_total[:, :, None])
        .astype(jnp.bfloat16)
        .reshape(row_count, head_count * V_DIM)
    )
    mixer_rows = jnp.concatenate([attention, conv_result], axis=1)
    out_weight = jnp.concatenate([out_heads, out_conv], axis=0)
    partial_sum = jnp.dot(mixer_rows, out_weight, preferred_element_type=jnp.float32)
    mixed = over_pieces(partial_sum.astype(jnp.bfloat16), "tp").astype(jnp.float32)
    return mixed.astype(jnp.bfloat16)[None]


def solution(mesh):
    in_specs = (
        P("fs", "sp", None),
        P(),
        P("fs", "tp"),
        P("fs", "tp"),
        P(),
        P("fs", "tp"),
        P("fs", "tp"),
        P("fs", "tp"),
        P(),
        P(),
        P(),
        P(),
        P("fs", "tp"),
        P("fs", "tp"),
        P(None, "tp"),
        P("tp"),
        P("tp"),
        P("tp", "fs"),
        P("tp", "fs"),
    )
    out_specs = P("fs", "sp", None)
    return jax.shard_map(local, mesh=mesh, in_specs=in_specs, out_specs=out_specs, check_vma=False)
```

profile of v0, /device:TPU:1, one launch (start us, length us, event | category | flops | bytes accessed | tf_op | source)
XLA Modules:
  0.0 266.6 jit_solution(5219154865961062994)
XLA Ops:
  6.5 1.1 copy.74
  7.6 1.0 copy.75
  8.6 2.1 pad_maximum_fusion
  10.8 1.9 copy.76
  12.7 0.8 mul.322
  13.4 0.8 pad_maximum_fusion.8
  14.2 10.7 %all_gather.30 = bf16[512,256]{1,0:T(8,128)(2,1)S(1)} all-gather(bf16[128,256]{1,0:T(8,128)(2,1)S(1)} %pad_maximum_fusion.8), channel_id=1, replica_groups=mesh['sp'=16,'fs'=4,'tp'=8] {'fs'}, dimensions={0}, use_global_device_ids=true | all-gather | bytes 327680 | tf_op jit(solution)/shard_map/all_gather | solution.py:25
  24.9 0.7 copy-done.1
  25.8 0.8 mul.347
  26.5 9.8 %all_gather.32 = bf16[768,192]{1,0:T(8,128)(2,1)S(1)} all-gather(bf16[192,192]{1,0:T(8,128)(2,1)} %param.28), channel_id=1, replica_groups=mesh['sp'=16,'fs'=4,'tp'=8] {'fs'}, dimensions={0}, use_global_device_ids=true | all-gather | bytes 368640 | tf_op jit(solution)/shard_map/all_gather | solution.py:168
  37.0 19.0 %all-gather.7.cloned.1.call-done = bf16[2048,416]{1,0:T(8,128)(2,1)} async-done(((bf16[512,416]{1,0:T(8,128)(2,1)}), bf16[2048,416]{1,0:T(8,128)(2,1)}) %all-gather.7.cloned.1.call-update) | async-done | bytes 1703952 | tf_op jit(solution)/shard_map/all_gather | solution.py:25
  56.0 2.0 split.29
  58.0 2.7 %fusion.51 = (bf16[256,448]{0,1:T(8,128)(2,1)S(1)}, f32[256,448]{0,1:T(8,128)}) fusion(bf16[2048,256]{1,0:T(8,128)(2,1)S(1)} %split.29, bf16[2048,32]{1,0:T(8,128)(2,1)S(1)} %copy-done.4, bf16[2048,160]{1,0:T(8,128)(2,1)S(1)} %slice-done.1, bf16[1,256,2048]{2,1,0:T(8,128)(2,1)S(1)} %copy-done.3, f32[2048]{0:T(1024)S(1)} %copy-done.9, ...), kind=kOutput, calls=%fused_computation.114 | convolution fusion | flops 477478912 | bytes 3580928 | tf_op jit(solution)/shard_map/dot_general | solution.py:178
  61.2 13.9 %all-gather = bf16[327680]{0:T(1024)(128)(2,1)S(1)} all-gather(bf16[40960]{0:T(1024)(128)(2,1)S(1)} %pad_maximum_fusion.7), channel_id=2, replica_groups=mesh['sp'=16,'fs'=4,'tp'=8] {'tp'}, dimensions={0}, use_global_device_ids=true | all-gather | bytes 737280 | tf_op jit(solution)/shard_map/all_gather | solution.py:36
  78.2 0.8 multiply_multiply_fusion
  80.5 1.0 fusion.47
  81.6 2.9 %collective-permute-start = (bf16[30,128]{0,1:T(8,128)(2,1)S(1)}, bf16[30,128]{0,1:T(8,128)(2,1)S(1)}, u32[]{:S(2)}, u32[]{:S(2)}) collective-permute-start(bf16[30,128]{0,1:T(8,128)(2,1)S(1)} %slice.91), channel_id=1, source_target_pairs={{0,32},{32,64},{64,96},{96,128},{128,160},{160,192},{192,224},{224... | collective-permute-start | bytes 23048 | tf_op jit(solution)/shard_map/ppermute | solution.py:47
  84.6 1.6 pad_maximum_fusion.1
  86.4 30.1 %while.35 = (s32[]{:T(128)}, f32[256,128]{1,0:T(8,128)S(1)}, bf16[286,128]{0,1:T(8,128)(2,1)S(1)}, bf16[31,128]{1,0:T(8,128)(2,1)}, s32[]{:T(128)}, /*index=5*/s32[]{:T(128)}) while((s32[]{:T(128)}, f32[256,128]{1,0:T(8,128)S(1)}, bf16[286,128]{0,1:T(8,128)(2,1)S(1)}, bf16[31,128]{1,0:T(8,128)(2,1)}, s32[]{:T(128)}, ...), condition=%wide.region_10.11_spmd.clone, body=%wide.region_9.10_spmd.clone.sunk | while | flops 131203 | bytes 591191 | solution.py:131
  86.6 0.7 bitcast_convert_fusion.2
  87.6 0.7 bitcast_convert_fusion.2
  88.6 0.7 bitcast_convert_fusion.2
  89.5 0.7 bitcast_convert_fusion.2
  90.5 0.7 bitcast_convert_fusion.2
  91.5 0.7 bitcast_convert_fusion.2
  92.4 0.7 bitcast_convert_fusion.2
  93.4 0.7 bitcast_convert_fusion.2
  94.4 0.7 bitcast_convert_fusion.2
  95.4 0.7 bitcast_convert_fusion.2
  96.3 0.7 bitcast_convert_fusion.2
  97.3 0.7 bitcast_convert_fusion.2
  98.3 0.7 bitcast_convert_fusion.2
  99.2 0.7 bitcast_convert_fusion.2
  100.2 0.7 bitcast_convert_fusion.2
  101.2 0.7 bitcast_convert_fusion.2
  102.2 0.7 bitcast_convert_fusion.2
  103.1 0.7 bitcast_convert_fusion.2
  104.1 0.7 bitcast_convert_fusion.2
  105.1 0.7 bitcast_convert_fusion.2
  106.0 0.7 bitcast_convert_fusion.2
  107.0 0.7 bitcast_convert_fusion.2
  108.0 0.7 bitcast_convert_fusion.2
  109.0 0.7 bitcast_convert_fusion.2
  109.9 0.7 bitcast_convert_fusion.2
  110.9 0.7 bitcast_convert_fusion.2
  112.8 0.7 bitcast_convert_fusion.2
  113.8 0.7 bitcast_convert_fusion.2
  114.8 0.7 bitcast_convert_fusion.2
  115.8 0.7 bitcast_convert_fusion.2
  117.3 4.1 %all-to-all-start = ((f32[8,1,512]{2,1,0:T(1,128)}), f32[8,1,512]{2,1,0:T(1,128)S(1)}, u32[]{:S(2)}, u32[]{:S(2)}) async-start(f32[8,1,512]{2,1,0:T(1,128)} %broadcast_in_dim.109), calls=%async_computation | async-start | bytes 32768 | tf_op jit(solution)/shard_map/all_to_all | solution.py:52
  121.5 4.5 %all-to-all-done = f32[8,1,512]{2,1,0:T(1,128)S(1)} async-done(((f32[8,1,512]{2,1,0:T(1,128)}), f32[8,1,512]{2,1,0:T(1,128)S(1)}, u32[]{:S(2)}, u32[]{:S(2)}) %all-to-all-start) | async-done | bytes 16416 | tf_op jit(solution)/shard_map/all_to_all | solution.py:52
  126.2 25.2 %all-gather.9.cloned.1.call-done = bf16[4096,320]{0,1:T(8,128)(2,1)} async-done(((bf16[256,320]{0,1:T(8,128)(2,1)}), bf16[4096,320]{0,1:T(8,128)(2,1)}) %all-gather.9.cloned.1.call-update) | async-done | bytes 2621456 | tf_op jit(solution)/shard_map/all_gather | solution.py:25
  151.5 1.6 split.32
  153.2 16.1 %while.34 = (s32[]{:T(128)}, f32[256,2]{0,1:T(2,128)S(1)}, f32[256,2]{0,1:T(2,128)S(1)}, f32[256,2,64]{0,2,1:T(8,128)S(1)}, bf16[4096,192]{0,1:T(8,128)(2,1)S(1)...) while((s32[]{:T(128)}, f32[256,2]{0,1:T(2,128)S(1)}, ...), condition=%wide.region_8.9_spmd.clone, body=%wide.region_5.0_spmd.clone.sunk | while | flops 349837824 | bytes 35801304 | solution.py:261
  153.7 2.8 %fusion.75 = (f32[256,2]{0,1:T(2,128)S(1)}, f32[2,2048,256]{2,1,0:T(8,128)}) fusion(pred[256,2048]{0,1:T(8,128)(4,1)S(1)} %broadcast_compare_fusion.2, bf16[2048,2,96]{0,2,1:T(8,128)(2,1)S(1)} %bitcast.88, bf16[256,2,96]{0,2,1:T(8,128)(2,1)S(1)} %get-tuple-element.527), kind=kOutput, calls=%fused_computation.3.clone.1 | convolution fusion | flops 204471808 | bytes 5605376 | tf_op jit(solution)/shard_map/while/body/eval_jaxpr/qhd,khd->qhk/dot_general | solution.py:214
  156.6 3.4 %fusion.77 = f32[256,2]{0,1:T(2,128)S(1)} fusion(f32[2,2048,256]{2,1,0:T(8,128)} %get-tuple-element.473, f32[256,2]{0,1:T(2,128)S(1)} %fusion.76, pred[256,2048]{0,1:T(8,128)(4,1)S(1)} %broadcast_compare_fusion.2), kind=kLoop, calls=%fused_computation.5.clone.1 | loop fusion | flops 5242368 | bytes 4722688 | tf_op jit(solution)/shard_map/while/body/eval_jaxpr/reduce_sum | solution.py:222
  160.1 1.1 fusion.79
  161.8 2.8 %fusion.75 = (f32[256,2]{0,1:T(2,128)S(1)}, f32[2,2048,256]{2,1,0:T(8,128)}) fusion(pred[256,2048]{0,1:T(8,128)(4,1)S(1)} %broadcast_compare_fusion.2, bf16[2048,2,96]{0,2,1:T(8,128)(2,1)S(1)} %bitcast.88, bf16[256,2,96]{0,2,1:T(8,128)(2,1)S(1)} %get-tuple-element.527), kind=kOutput, calls=%fused_computation.3.clone.1 | convolution fusion | flops 204471808 | bytes 5605376 | tf_op jit(solution)/shard_map/while/body/eval_jaxpr/qhd,khd->qhk/dot_general | solution.py:214
  164.6 3.4 %fusion.77 = f32[256,2]{0,1:T(2,128)S(1)} fusion(f32[2,2048,256]{2,1,0:T(8,128)} %get-tuple-element.473, f32[256,2]{0,1:T(2,128)S(1)} %fusion.76, pred[256,2048]{0,1:T(8,128)(4,1)S(1)} %broadcast_compare_fusion.2), kind=kLoop, calls=%fused_computation.5.clone.1 | loop fusion | flops 5242368 | bytes 4722688 | tf_op jit(solution)/shard_map/while/body/eval_jaxpr/reduce_sum | solution.py:222
  168.2 1.1 fusion.79
  169.3 21.4 %all-gather.11.cloned.1.call-done = bf16[256,2048]{1,0:T(8,128)(2,1)} async-done(((bf16[256,512]{1,0:T(8,128)(2,1)}), bf16[256,2048]{1,0:T(8,128)(2,1)}) %all-gather.11.cloned.1.call-update) | async-done | bytes 1048592 | tf_op jit(solution)/shard_map/all_gather | solution.py:25
  190.7 2.7 convolution_convert_fusion
  193.4 60.4 %all-gather.13.cloned.1.call-done = bf16[2048,2048]{1,0:T(8,128)(2,1)} async-done(((bf16[256,2048]{1,0:T(8,128)(2,1)}), bf16[2048,2048]{1,0:T(8,128)(2,1)}) %all-gather.13.cloned.1.call-update) | async-done | bytes 8388624 | tf_op jit(solution)/shard_map/all_gather | solution.py:70
  253.7 6.4 %reduce_sum.108 = bf16[256,2048]{1,0:T(8,128)(2,1)} reduce(bf16[8,256,2048]{2,1,0:T(8,128)(2,1)} %bitcast.91, bf16[]{:T(256)} %constant.206.clone.1), dimensions={0}, to_apply=%region_14.15 | reduce | flops 3670016 | bytes 9437186 | tf_op jit(solution)/shard_map/reduce_sum | solution.py:70
  (202 shorter events, 16.7 us)
Async XLA Ops:
  6.5 30.0 %copy-start.3 = (bf16[1,256,2048]{2,1,0:T(8,128)(2,1)S(1)}, bf16[1,256,2048]{2,1,0:T(8,128)(2,1)}, u32[]{:S(2)}) copy-start(bf16[1,256,2048]{2,1,0:T(8,128)(2,1)} %param.23) | copy-start | bytes 3145732
  6.5 49.5 %all-gather.7.cloned.1.call-start = ((), (), s32[]{:S(2)}) async-start(), calls=%async_computation.1 | async-start | bytes 2621440 | tf_op jit(solution)/shard_map/all_gather | solution.py:25
  10.7 47.3 %copy-start.9 = (f32[2048]{0:T(1024)S(1)}, f32[2048]{0:T(1024)}, u32[]{:S(2)}) copy-start(f32[2048]{0:T(1024)} %param.24) | copy-start | bytes 24580
  10.7 140.8 %all-gather.9.cloned.1.call-start = ((), (), s32[]{:S(2)}) async-start(), calls=%async_computation.2 | async-start | bytes 2785280 | tf_op jit(solution)/shard_map/all_gather | solution.py:25
  24.9 0.7 copy-start.1
  56.0 2.0 slice-start.1
  56.0 2.0 copy-start.4
  76.8 2.5 copy-start.6
  77.3 2.2 copy-start.2
  77.5 7.1 %copy-start.5 = (bf16[128,512]{1,0:T(8,128)(2,1)S(1)}, bf16[128,512]{1,0:T(8,128)(2,1)}, u32[]{:S(2)}) copy-start(bf16[128,512]{1,0:T(8,128)(2,1)} %param.41) | copy-start | bytes 393220
  79.0 47.1 %copy-start.7 = (f32[128]{0:T(128)S(1)}, f32[128]{0:T(128)}, u32[]{:S(2)}) copy-start(f32[128]{0:T(128)} %param.39) | copy-start | bytes 1540
  79.0 47.1 %copy-start.8 = (f32[128]{0:T(128)S(1)}, f32[128]{0:T(128)}, u32[]{:S(2)}) copy-start(f32[128]{0:T(128)} %param.38) | copy-start | bytes 1540
  80.5 110.2 %all-gather.11.cloned.1.call-start = ((), (), s32[]{:S(2)}) async-start(), calls=%async_computation.3 | async-start | bytes 1310720 | tf_op jit(solution)/shard_map/all_gather | solution.py:25
  81.6 4.7 %collective-permute-start = (bf16[30,128]{0,1:T(8,128)(2,1)S(1)}, bf16[30,128]{0,1:T(8,128)(2,1)S(1)}, u32[]{:S(2)}, u32[]{:S(2)}) collective-permute-start(bf16[30,128]{0,1:T(8,128)(2,1)S(1)} %slice.91), channel_id=1, source_target_pairs={{0,32},{32,64},{64,96},{96,128},{128,160},{160,192},{192,224},{224... | collective-permute-start | bytes 23048 | tf_op jit(solution)/shard_map/ppermute | solution.py:47
  117.3 8.8 %all-to-all-start = ((f32[8,1,512]{2,1,0:T(1,128)}), f32[8,1,512]{2,1,0:T(1,128)S(1)}, u32[]{:S(2)}, u32[]{:S(2)}) async-start(f32[8,1,512]{2,1,0:T(1,128)} %broadcast_in_dim.109), calls=%async_computation | async-start | bytes 32768 | tf_op jit(solution)/shard_map/all_to_all | solution.py:52
  121.4 132.3 %all-gather.13.cloned.1.call-start = ((), (), s32[]{:S(2)}) async-start(), calls=%async_computation.4 | async-start | bytes 9437184 | tf_op jit(solution)/shard_map/all_gather | solution.py:70
  151.5 1.7 slice-start
  156.6 3.5 %copy-start = (f32[2,2048,256]{2,1,0:T(8,128)S(1)}, f32[2,2048,256]{2,1,0:T(8,128)}, u32[]{:S(2)}) copy-start(f32[2,2048,256]{2,1,0:T(8,128)} %get-tuple-element.473) | copy-start | bytes 12582916 | tf_op jit(solution)/shard_map/while
  164.6 3.5 %copy-start = (f32[2,2048,256]{2,1,0:T(8,128)S(1)}, f32[2,2048,256]{2,1,0:T(8,128)}, u32[]{:S(2)}) copy-start(f32[2,2048,256]{2,1,0:T(8,128)} %get-tuple-element.473) | copy-start | bytes 12582916 | tf_op jit(solution)/shard_map/while
Sparse Core Ops, SparseCore 0:
  10.8 45.1 all-gather.6
  80.6 70.8 all-gather.8
  153.6 37.0 all-gather.10
  193.5 60.1 all-gather.12
where the time goes:
time: 268 us; the launch traced here: 267 us
  waiting for transfers between devices  131 us (49%)
  other arithmetic  46.1 us (17%)
  blocking collectives  34.5 us (13%)
  local copies, waits for them, and re-layouts  19.8 us (7%)
  matrix products  13.8 us (5%)
  between operations  13.6 us (5%)
  starting transfers between devices  7.13 us (3%)
    all_gather x3, waiting for transfers between devices, side_by_side(): lax.all_gather(both, axis, axis=dim, tiled=True)  65.6 us
    all_gather x1, waiting for transfers between devices, over_pieces(): return lax.all_gather(value, axis).astype(jnp.float32).sum(0)  60.4 us
    mul x31, other arithmetic, add_tap(): return running + window * weight_row  21.5 us
    all_gather x1, blocking collectives, one_gather(): lines, at, outs = (lax.all_gather(vector, axis), 0, [])  13.9 us
    all_gather x1, blocking collectives, side_by_side(): lax.all_gather(both, axis, axis=dim, tiled=True)  10.7 us
    all_gather x1, blocking collectives, local(): lax.all_gather(query_up, 'fs', axis=0, tiled=True)  9.83 us
    reduce_sum x2, other arithmetic, attend(): row_total = row_total * factor + jnp.sum(weights, axis=2)  6.89 us
    reduce_sum x1, other arithmetic, over_pieces(): return lax.all_gather(value, axis).astype(jnp.float32).sum(0)  6.39 us
  transfers between devices with their start and end apart: 6, of which 5 were waited for; matrix products, arithmetic and copies ran while one was open for 21% of the time, Pallas kernels for 0%

commit v1 on v0

v1 whole, which is shorter than its diff:
```python
import jax
import jax.numpy as jnp
from jax import lax
from jax.experimental import pallas as pl
from jax.experimental.pallas import tpu as pltpu
from jax.sharding import PartitionSpec as P

QK_NOPE = 64
QK_ROPE = 32
V_DIM = 64
CONV_W = 1024
SEG = 64
QK_DIM = 96
Q_LAT = 768
KV_LAT = 512
ROWS = 256
TAPS = 31
HALO = 32
LANES = 128
N_FS = 4
N_TP = 8
N_SP = 16
CHUNK = 512

epsilon = 1e-06
rope_base = 10000.0
masked_score = -1e30
log2_e = 1.4426950408889634
bf16 = jnp.bfloat16
f32 = jnp.float32

SAME_CORE = [[0, 2, 4, 6], [1, 3, 5, 7]]
CORE_PAIRS = [(i, i ^ 1) for i in range(N_TP)]


def call(kernel, out_shape, scratch=(), scalars=0, arrays=0):
    specs = {}
    if scalars:
        smem = pl.BlockSpec(memory_space=pltpu.SMEM)
        specs["in_specs"] = [smem] * scalars + [pl.BlockSpec(memory_space=pltpu.VMEM)] * arrays
    return pl.pallas_call(
        kernel,
        out_shape=out_shape,
        **specs,
        scratch_shapes=list(scratch),
        compiler_params=pltpu.CompilerParams(vmem_limit_bytes=48 * 1024 * 1024),
    )


def norm_rows(matrix, scale_vector):
    return (
        matrix
        * lax.rsqrt(jnp.mean(matrix * matrix, axis=-1, keepdims=True) + epsilon)
        * scale_vector
    )


def head_tile(tile, gain, cosine, sine_up, sine_down):
    scale = lax.rsqrt(jnp.sum(tile * tile, axis=-1, keepdims=True) * (1.0 / QK_DIM) + epsilon)
    tile = tile * scale * gain
    half = QK_ROPE // 2
    return (
        tile * cosine
        + pltpu.roll(tile, LANES - half, 1) * sine_up
        + pltpu.roll(tile, half, 1) * sine_down
    )


def keys_values_kernel(lat_ref, rope_ref, w_ref, mgain_ref, kgain_ref, cos_ref, up_ref, down_ref, out_ref, m_scr, w_scr):
    total = jnp.zeros((ROWS, 1), f32)
    for g in range(N_TP):
        piece = lat_ref[g, :, :64].astype(f32)
        total = total + jnp.sum(piece * piece, axis=-1, keepdims=True)
    scale = lax.rsqrt(total * (1.0 / KV_LAT) + epsilon)
    for g in range(N_TP):
        piece = lat_ref[g, :, :64].astype(f32)
        cols = slice(g * 64, (g + 1) * 64)
        m_scr[:, cols] = (piece * scale * mgain_ref[:, cols]).astype(bf16)
    for f in range(N_FS):
        for b in range(4):
            w_scr[f * 128 : (f + 1) * 128, b * 64 : (b + 1) * 64] = w_ref[
                f, b * 128 : (b + 1) * 128, :64
            ]
    both = jnp.dot(m_scr[...], w_scr[...], preferred_element_type=f32)
    nope = both[:, :LANES]
    lane = lax.broadcasted_iota(jnp.int32, (ROWS, LANES), 1)
    rope = rope_ref[...].astype(f32)
    for h in range(2):
        part = nope if h == 0 else pltpu.roll(nope, 64, 1)
        tile = jnp.where(lane < QK_NOPE, part, rope)
        out_ref[:, h * LANES : (h + 1) * LANES] = head_tile(
            tile, kgain_ref[...], cos_ref[...], up_ref[...], down_ref[...]
        ).astype(bf16)
    out_ref[:, 2 * LANES :] = both[:, LANES:].astype(bf16)


def queries_kernel(lat_ref, w_ref, lgain_ref, qgain_ref, cos_ref, up_ref, down_ref, out_ref, q_scr):
    total = jnp.zeros((ROWS, 1), f32)
    for g in range(N_TP):
        piece = lat_ref[g, :, 64:].astype(f32)
        total = total + jnp.sum(piece * piece, axis=-1, keepdims=True)
    scale = lax.rsqrt(total * (1.0 / Q_LAT) + epsilon)
    for g in range(N_TP):
        piece = lat_ref[g, :, 64:].astype(f32)
        cols = slice(g * 96, (g + 1) * 96)
        q_scr[:, cols] = (piece * scale * lgain_ref[:, cols]).astype(bf16)
    both = jnp.zeros((ROWS, 2 * LANES), f32)
    for f in range(N_FS):
        both = both + jnp.dot(
            q_scr[:, f * 192 : (f + 1) * 192], w_ref[f, 512:704, :], preferred_element_type=f32
        )
    for h in range(2):
        out_ref[:, h * LANES : (h + 1) * LANES] = head_tile(
            both[:, h * LANES : (h + 1) * LANES],
            qgain_ref[...],
            cos_ref[...],
            up_ref[...],
            down_ref[...],
        ).astype(bf16)


def gated_kernel(normed_ref, w_ref, out_ref):
    both = jnp.zeros((ROWS, 2 * LANES), f32)
    for f in range(N_FS):
        both = both + jnp.dot(
            normed_ref[:, f * 512 : (f + 1) * 512], w_ref[f, :512, :], preferred_element_type=f32
        )
    out_ref[...] = (both[:, :LANES] * jax.nn.sigmoid(both[:, LANES:])).astype(bf16)


def conv_kernel_body(halo_ref, gated_ref, taps_ref, sum_ref, first_ref, second_ref, ext_scr):
    ext_scr[:HALO, :] = halo_ref[...].astype(f32)
    ext_scr[HALO:, :] = gated_ref[...].astype(f32)
    start = HALO - (TAPS - 1)
    block = 64
    for r in range(0, ROWS, block):
        running = jnp.zeros((block, LANES), f32)
        for j in range(TAPS):
            running = running + ext_scr[pl.ds(r + start + j, block), :] * taps_ref[j : j + 1, :]
        sum_ref[r : r + block, :] = running
        total = jnp.sum(running, axis=-1, keepdims=True)
        off = running - total * (1.0 / LANES)
        first_ref[r : r + block, :] = total
        second_ref[r : r + block, :] = jnp.sum(off * off, axis=-1, keepdims=True)


def attention_kernel(at_ref, q_ref, kv_ref, conv_ref, heads_ref, conv_w_ref, out_ref):
    at = at_ref[0]
    rate = QK_DIM ** (-0.5) * log2_e
    heads = [q_ref[:, h * LANES : (h + 1) * LANES] for h in range(2)]

    def part(state, chunk, mask):
        block = pl.multiple_of(chunk * CHUNK, CHUNK)
        values = kv_ref[pl.ds(block, CHUNK), 2 * LANES :]
        fresh = []
        for h in range(2):
            top, total, weighted = state[h]
            keys = kv_ref[pl.ds(block, CHUNK), h * LANES : (h + 1) * LANES]
            scores = lax.dot_general(
                heads[h], keys, (((1,), (1,)), ((), ())), preferred_element_type=f32
            ) * rate
            if mask is not None:
                scores = jnp.where(mask, scores, masked_score)
            new_top = jnp.maximum(top, jnp.max(scores, axis=-1, keepdims=True))
            weights = jnp.exp2(scores - new_top)
            factor = jnp.exp2(top - new_top)
            total = total * factor + jnp.sum(weights, axis=-1, keepdims=True)
            weighted = weighted * factor + jnp.dot(
                weights.astype(bf16), values, preferred_element_type=f32
            )
            fresh.append((new_top, total, weighted))
        return tuple(fresh)

    last = at // (CHUNK // ROWS)
    row = lax.broadcasted_iota(jnp.int32, (ROWS, CHUNK), 0) + at * ROWS
    col = lax.broadcasted_iota(jnp.int32, (ROWS, CHUNK), 1) + last * CHUNK
    mask = jnp.right_shift(col, 6) <= jnp.right_shift(row, 6)
    empty = (
        jnp.full((ROWS, 1), masked_score, f32),
        jnp.zeros((ROWS, 1), f32),
        jnp.zeros((ROWS, LANES), f32),
    )
    state = part((empty, empty), last, mask)
    state = lax.fori_loop(0, last, lambda c, s: part(s, c, None), state)
    lane = lax.broadcasted_iota(jnp.int32, (ROWS, LANES), 1)
    result = jnp.where(
        lane < V_DIM, state[0][2] / state[0][1], state[1][2] / state[1][1]
    ).astype(bf16)
    conv = conv_ref[...]
    for f in range(N_FS):
        out_ref[:, f * 512 : (f + 1) * 512] = (
            jnp.dot(result, heads_ref[f], preferred_element_type=f32)
            + jnp.dot(conv, conv_w_ref[f], preferred_element_type=f32)
        ).astype(bf16)


def rotation_tables(positions):
    inverse_freq = 1.0 / rope_base ** (jnp.arange(0, QK_ROPE, 2, dtype=f32) / QK_ROPE)
    angles = positions.astype(f32)[:, None] * inverse_freq[None, :]
    cosine, sine = jnp.cos(angles), jnp.sin(angles)
    rows = positions.shape[0]
    ones = jnp.ones((rows, QK_NOPE), f32)
    zeros = jnp.zeros((rows, QK_NOPE), f32)
    pad = jnp.zeros((rows, LANES - QK_DIM), f32)
    none = jnp.zeros_like(sine)
    return (
        jnp.concatenate([ones, cosine, cosine, pad], axis=1),
        jnp.concatenate([zeros, -sine, none, pad], axis=1),
        jnp.concatenate([zeros, none, sine, pad], axis=1),
    )


def local(
    tokens,
    mix_gain,
    query_down,
    memory_down,
    rope_weight,
    query_up,
    key_up,
    value_up,
    latent_gain,
    memory_gain,
    query_gain,
    key_gain,
    conv_value,
    conv_gate,
    conv_kernel,
    channel_gain,
    channel_shift,
    heads_out,
    conv_out,
):
    at = lax.axis_index("sp")
    query_pad = jnp.pad(query_up.reshape(192, 2, QK_DIM), ((0, 0), (0, 0), (0, 32))).reshape(192, 256)
    wide = jnp.concatenate([jnp.concatenate([conv_value, conv_gate], axis=1), query_pad], axis=0)
    wide_all = lax.all_gather(wide, "fs")
    up = jnp.concatenate(
        [key_up[:, :64], key_up[:, 64:], value_up[:, :64], value_up[:, 64:]], axis=0
    )
    narrow = jnp.concatenate([up, memory_down, query_down], axis=1)
    normed = norm_rows(tokens[0].astype(f32), mix_gain).astype(bf16)
    rope_pad = jnp.pad(rope_weight, ((0, 0), (QK_NOPE, LANES - QK_DIM)))
    rope_rows = jnp.dot(normed, rope_pad, preferred_element_type=f32).astype(bf16)
    narrow_all = lax.all_gather(narrow, "fs")
    projected = jnp.dot(
        normed, narrow_all.reshape(2048, 224), preferred_element_type=f32
    ).astype(bf16)
    latents = lax.all_gather(projected[:, 64:], "tp")
    positions = at * ROWS + jnp.arange(ROWS, dtype=jnp.int32)
    cosine, sine_up, sine_down = rotation_tables(positions)

    def row(vector, width):
        return jnp.pad(vector, (0, width - vector.shape[0]))[None, :]

    own = call(
        keys_values_kernel,
        jax.ShapeDtypeStruct((ROWS, 3 * LANES), bf16),
        [pltpu.VMEM((ROWS, KV_LAT), bf16), pltpu.VMEM((KV_LAT, 256), bf16)],
    )(
        latents, rope_rows, narrow_all, memory_gain[None, :], row(key_gain, LANES),
        cosine, sine_up, sine_down,
    )
    pieces = lax.all_gather(own, "sp", axis=0, tiled=True)
    queries = call(
        queries_kernel,
        jax.ShapeDtypeStruct((ROWS, 2 * LANES), bf16),
        [pltpu.VMEM((ROWS, Q_LAT), bf16)],
    )(
        latents, wide_all, latent_gain[None, :], row(query_gain, LANES),
        cosine, sine_up, sine_down,
    )
    gated = call(gated_kernel, jax.ShapeDtypeStruct((ROWS, LANES), bf16))(normed, wide_all)
    halo = lax.ppermute(gated[ROWS - HALO :], "sp", [(i, i + 1) for i in range(N_SP - 1)])
    taps = jnp.pad(conv_kernel.astype(f32), ((0, 1), (0, 0)))
    column = jax.ShapeDtypeStruct((ROWS, 1), f32)
    conv_sum, first, second = call(
        conv_kernel_body,
        (jax.ShapeDtypeStruct((ROWS, LANES), f32), column, column),
        [pltpu.VMEM((ROWS + HALO, LANES), f32)],
    )(halo, gated, taps)
    stats = jnp.concatenate([first[:, 0], second[:, 0]])
    stats = jnp.broadcast_to(stats, (N_TP, 1, 2 * ROWS))
    stats = lax.all_to_all(stats, "tp", split_axis=0, concat_axis=0, tiled=True)[:, 0]
    sums, squares = stats[:, :ROWS], stats[:, ROWS:]
    row_mean = jnp.sum(sums, axis=0) * (1.0 / CONV_W)
    apart = sums * (1.0 / LANES) - row_mean[None, :]
    spread = jnp.sum(squares + LANES * apart * apart, axis=0) * (1.0 / CONV_W)
    conv_result = jax.nn.silu(
        (conv_sum - row_mean[:, None]) * lax.rsqrt(spread + epsilon)[:, None] * channel_gain
        + channel_shift
    ).astype(bf16)
    heads_all = lax.all_gather(heads_out, "fs")
    conv_all = lax.all_gather(conv_out, "fs")
    partial = call(
        attention_kernel, jax.ShapeDtypeStruct((ROWS, 2048), bf16), scalars=1, arrays=5
    )(at[None], queries, pieces, conv_result, heads_all, conv_all)
    share = lax.all_to_all(
        partial.reshape(N_TP, ROWS // N_TP, 2048), "tp", split_axis=0, concat_axis=0, tiled=True
    )
    share = jnp.sum(share.astype(f32), axis=0).astype(bf16)
    mine = lax.all_gather(share, "tp", axis_index_groups=SAME_CORE)
    other = lax.ppermute(mine, "tp", CORE_PAIRS)
    even = lax.axis_index("tp") % 2 == 0
    mixed = jnp.stack([jnp.where(even, mine, other), jnp.where(even, other, mine)], axis=1)
    return mixed.reshape(1, ROWS, 2048)


def solution(mesh):
    in_specs = (
        P("fs", "sp", None),
        P(),
        P("fs", "tp"),
        P("fs", "tp"),
        P(),
        P("fs", "tp"),
        P("fs", "tp"),
        P("fs", "tp"),
        P(),
        P(),
        P(),
        P(),
        P("fs", "tp"),
        P("fs", "tp"),
        P(None, "tp"),
        P("tp"),
        P("tp"),
        P("tp", "fs"),
        P("tp", "fs"),
    )
    out_specs = P("fs", "sp", None)
    return jax.shard_map(local, mesh=mesh, in_specs=in_specs, out_specs=out_specs, check_vma=False)
```

time: 268 us -> 178 us (0.66)
  waiting for transfers between devices: 131 us -> 18.4 us
  blocking collectives: 34.5 us -> 94.8 us
  other arithmetic: 46.1 us -> 9.03 us
  matrix products: 13.8 us -> 1.96 us
  starting transfers between devices: 7.13 us -> 17.5 us
  Pallas kernels: 0 us -> 7.05 us
  local copies, waits for them, and re-layouts: 19.8 us -> 14.9 us
    all_gather x4 -> x2, waiting for transfers between devices: 126 us -> 16.1 us  [the longest x1 16.1 us: local(): pieces = lax.all_gather(own, 'sp', axis=0, tiled=True)]
    all_gather x3 -> x5, blocking collectives: 34.5 us -> 66.1 us  [the longest x1 21.2 us: local(): latents = lax.all_gather(projected[:, 64:], 'tp')]
    all_to_all x0 -> x1, blocking collectives: none -> 28.6 us  [local(): lax.all_to_all(partial.reshape(N_TP, ROWS // N_TP, 2048), 'tp', split_axi...]
    mul x33 -> x1, other arithmetic: 22.4 us -> 0.01 us  [local(): row_mean = jnp.sum(sums, axis=0) * (1.0 / CONV_W)]
    reduce_sum x5 -> x3, other arithmetic: 13.5 us -> 0.19 us  [the longest x1 0.15 us: local(): share = jnp.sum(share.astype(f32), axis=0).astype(bf16)]
    dot_general x9 -> x2, matrix products: 13.8 us -> 1.96 us  [the longest x1 1.37 us: local(): jnp.dot(normed, rope_pad, preferred_element_type=f32).astype(bf16)]
    pallas_call x0 -> x5, Pallas kernels: none -> 7.05 us  [the longest x1 2.39 us: local(): call(queries_kernel, jax.ShapeDtypeStruct((ROWS, 2 * LANES), bf16), [pltp...]
    dynamic_slice x66 -> x0, local copies, waits for them, and re-layouts: 6.55 us -> none  [the longest x62 6.35 us: add_tap(): lax.dynamic_slice_in_dim(extended, tap_index, row_count, 0)]
  transfers between devices with their start and end apart: 6 -> 5, of which waited for: 5 -> 3; matrix products, arithmetic and copies ran while one was open for 21% -> 7% of each run, Pallas kernels for 0% -> 3%
where the time goes in v1:
time: 178 us; the launch traced here: 177 us
  blocking collectives  94.8 us (53%)
  waiting for transfers between devices  18.4 us (10%)
  starting transfers between devices  17.5 us (10%)
  local copies, waits for them, and re-layouts  14.9 us (8%)
  between operations  13.8 us (8%)
  other arithmetic  9.03 us (5%)
  Pallas kernels  7.05 us (4%)
  matrix products  1.96 us (1%)
    all_to_all x1, blocking collectives, local(): lax.all_to_all(partial.reshape(N_TP, ROWS // N_TP, 2048), 'tp', split_axi...  28.6 us
    all_gather x1, blocking collectives, local(): latents = lax.all_gather(projected[:, 64:], 'tp')  21.2 us
    all_gather x1, waiting for transfers between devices, local(): pieces = lax.all_gather(own, 'sp', axis=0, tiled=True)  16.1 us
    all_gather x1, blocking collectives, local(): narrow_all = lax.all_gather(narrow, 'fs')  12.8 us
    all_gather x1, blocking collectives, local(): conv_all = lax.all_gather(conv_out, 'fs')  11.1 us
    all_gather x1, blocking collectives, local(): heads_all = lax.all_gather(heads_out, 'fs')  11 us
    all_gather x1, blocking collectives, local(): mine = lax.all_gather(share, 'tp', axis_index_groups=SAME_CORE)  10.1 us
    all_to_all x1, starting transfers between devices, local(): lax.all_to_all(stats, 'tp', split_axis=0, concat_axis=0, tiled=True)[:, 0]  9.76 us
  transfers between devices with their start and end apart: 5, of which 3 were waited for; matrix products, arithmetic and copies ran while one was open for 7% of the time, Pallas kernels for 3%

profile of v1, /device:TPU:1, one launch (start us, length us, event | category | flops | bytes accessed | tf_op | source)
XLA Modules:
  0.0 177.4 jit_solution(17508938670012900855)
XLA Ops:
  6.5 0.0 all-gather.11.cloned.1.call-start
  6.5 1.1 reshape.65
  7.6 0.1 pad.21
  7.8 1.7 pad_maximum_fusion.1
  9.5 0.0 all-gather.11.cloned.1.call-update
  9.5 0.0 all-gather.9.cloned.1.call-start
  9.6 0.9 fusion.17
  10.6 0.1 copy.36
  10.7 0.0 copy-done.19
  10.7 0.0 copy-done.20
  10.7 0.0 copy-start.21
  10.7 12.8 %all-gather = bf16[2048,224]{0,1:T(8,128)(2,1)S(1)} all-gather(bf16[512,224]{0,1:T(8,128)(2,1)S(1)} %pad_maximum_fusion.2), channel_id=2, replica_groups=mesh['sp'=16,'fs'=4,'tp'=8] {'fs'}, dimensions={0}, use_global_device_ids=true | all-gather | bytes 1146880 | tf_op jit(solution)/shard_map/all_gather | solution.py:245
  23.5 0.0 copy-done.17
  23.5 0.3 fusion.2
  23.8 0.5 copy.39
  24.3 0.0 copy-done.21
  24.3 0.0 copy-start.23
  24.4 0.6 fusion.8
  25.0 21.2 %all-gather.1 = bf16[2048,160]{0,1:T(8,128)(2,1)S(1)} all-gather(bf16[256,160]{0,1:T(8,128)(2,1)S(1)} %slice.40), channel_id=3, replica_groups=mesh['sp'=16,'fs'=4,'tp'=8] {'tp'}, dimensions={0}, use_global_device_ids=true | all-gather | bytes 737280 | tf_op jit(solution)/shard_map/all_gather | solution.py:249
  46.2 0.5 copy.37
  46.7 0.1 pad.42.clone
  46.8 0.5 multiply_sine_fusion
  47.4 0.0 copy-start.16
  47.4 0.3 maximum_maximum_fusion.2
  47.7 1.7 fusion.4.normed_ref
  49.4 0.0 copy-start.18
  49.4 1.4 convolution_convert_fusion.rope_ref
  50.8 2.2 %shard_map.182 = bf16[256,384]{1,0:T(8,128)(2,1)} custom-call(bf16[8,256,160]{2,1,0:T(8,128)(2,1)S(1)} %bitcast.44, bf16[256,128]{1,0:T(8,128)(2,1)S(1)} %convolution_convert_fusion.rope_ref, bf16[4,512,224]{2,1,0:T(8,128)(2,1)S(1)} %bitcast.49, f32[1,512]{1,0:T(1,128)S(1)} %bitcast.52, f32[1,128]{1,0:T(1,128)S(1)} %pad_bitcast_fusion.kgain_ref, ...), custom_call_target="tpu_custom_call" | custom-call | tf_op jit(solution)/shard_map/pallas_call | solution.py:256
  53.0 0.0 all-gather.9.cloned.1.call-update
  53.1 11.0 %all-gather.3 = bf16[512,512]{1,0:T(8,128)(2,1)} all-gather(bf16[128,512]{1,0:T(8,128)(2,1)S(1)} %copy-done.18), channel_id=5, replica_groups=mesh['sp'=16,'fs'=4,'tp'=8] {'fs'}, dimensions={0}, use_global_device_ids=true | all-gather | bytes 655360 | tf_op jit(solution)/shard_map/all_gather | solution.py:293
  64.1 11.1 %all-gather.4 = bf16[512,512]{1,0:T(8,128)(2,1)} all-gather(bf16[128,512]{1,0:T(8,128)(2,1)} %param.37), channel_id=6, replica_groups=mesh['sp'=16,'fs'=4,'tp'=8] {'fs'}, dimensions={0}, use_global_device_ids=true | all-gather | bytes 655360 | tf_op jit(solution)/shard_map/all_gather | solution.py:294
  75.2 1.4 copy-done
  76.6 0.4 shard_map.183.gated_ref
  77.1 1.4 collective-permute-start
  78.5 0.8 collective-permute-done.halo_ref
  79.3 0.5 shard_map.184
  79.7 0.7 copy-done.13
  80.4 0.7 copy-done.14
  81.0 0.7 copy-done.15
  81.7 1.0 reduce.2
  82.7 1.0 reduce.1
  83.7 0.6 broadcast_in_dim.48
  84.4 9.8 %all-to-all-start = ((f32[8,1,512]{2,1,0:T(1,128)}), f32[8,1,512]{2,1,0:T(1,128)S(1)}, u32[]{:S(2)}, u32[]{:S(2)}) async-start(f32[8,1,512]{2,1,0:T(1,128)} %broadcast_in_dim.48), calls=%async_computation | async-start | bytes 32768 | tf_op jit(solution)/shard_map/all_to_all | solution.py:284
  94.1 0.7 pad_bitcast_fusion.1.qgain_ref
  94.8 0.7 broadcast_in_dim.40.lgain_ref
  95.5 0.9 copy-done.6
  96.4 0.9 copy-done.8
  97.3 0.9 copy-done.10
  98.2 2.4 %shard_map.181.q_ref = bf16[256,256]{1,0:T(8,128)(2,1)S(1)} custom-call(bf16[8,256,160]{2,1,0:T(8,128)(2,1)S(1)} %bitcast.45, bf16[4,704,256]{2,1,0:T(8,128)(2,1)S(1)} %bitcast.47, f32[1,768]{1,0:T(1,128)S(1)} %broadcast_in_dim.40.lgain_ref, f32[1,128]{1,0:T(1,128)S(1)} %pad_bitcast_fusion.1.qgain_ref, f32[256,128]{1,0:T(8,128)S(1)} %copy-done.10, ...), custom_call_target="tpu_custom_call" | custom-call | tf_op jit(solution)/shard_map/pallas_call | solution.py:265
  100.6 0.0 copy-start.11
  100.6 0.6 copy-done.11
  101.2 0.0 all-to-all-done
  101.3 1.1 multiply_convert_fusion.conv_ref
  102.4 16.1 %all-gather.9.cloned.1.call-done.kv_ref = bf16[4096,384]{1,0:T(8,128)(2,1)} async-done(((bf16[256,384]{1,0:T(8,128)(2,1)}), bf16[4096,384]{1,0:T(8,128)(2,1)}) %all-gather.9.cloned.1.call-update) | async-done | bytes 3145744 | tf_op jit(solution)/shard_map/all_gather | solution.py:264
  118.5 1.9 %copy-done.2 = bf16[4096,384]{1,0:T(8,128)(2,1)S(1)} copy-done((bf16[4096,384]{1,0:T(8,128)(2,1)S(1)}, bf16[4096,384]{1,0:T(8,128)(2,1)}, u32[]{:S(2)}) %copy-start.2) | copy-done | bytes 3145752
  120.4 0.9 copy-done.12
  121.3 1.5 shard_map.185
  122.8 28.6 %all_to_all.10 = bf16[8,32,2048]{2,1,0:T(8,128)(2,1)S(1)} all-to-all(bf16[8,32,2048]{2,1,0:T(8,128)(2,1)S(1)} %bitcast.48), channel_id=1, replica_groups=mesh['sp'=16,'fs'=4,'tp'=8] {'tp'}, dimensions={0} | all-to-all | bytes 2097152 | tf_op jit(solution)/shard_map/all_to_all | solution.py:298
  151.4 0.1 reduce_sum.42
  151.6 10.1 %all-gather.5 = bf16[128,2048]{1,0:T(8,128)(2,1)S(1)} all-gather(bf16[32,2048]{1,0:T(8,128)(2,1)S(1)} %reduce_sum.42), channel_id=7, replica_groups={{0,2,4,6},{1,3,5,7},{8,10,12,14},{9,11,13,15},{16,18,20,22},{17,19,21,2..., dimensions={0}, use_global_device_ids=true | all-gather | bytes 655360 | tf_op jit(solution)/shard_map/all_gather | solution.py:302
  161.7 6.3 %collective-permute-start.1 = (bf16[4,32,2048]{2,1,0:T(8,128)(2,1)S(1)}, bf16[4,32,2048]{2,1,0:T(8,128)(2,1)S(1)}, u32[]{:S(2)}, u32[]{:S(2)}) collective-permute-start(bf16[4,32,2048]{2,1,0:T(8,128)(2,1)S(1)} %bitcast.53), channel_id=1, source_target_pairs={{0,1},{1,0},{2,3},{3,2},{4,5},{5,4},{6,7},{7,6},{8,9},{9,8},{10,11... | collective-permute-start | bytes 1572872 | tf_op jit(solution)/shard_map/ppermute | solution.py:303
  167.9 1.5 collective-permute-done.1
  169.4 0.1 select_bitcast_fusion.1
  169.5 1.1 pad_maximum_fusion
  (52 shorter events, 0.3 us)
Async XLA Ops:
  6.5 4.1 %copy-start.19 = (bf16[512,96]{0,1:T(8,128)(2,1)S(1)}, bf16[512,96]{0,1:T(8,128)(2,1)}, u32[]{:S(2)}) copy-start(bf16[512,96]{0,1:T(8,128)(2,1)} %param.21) | copy-start | bytes 294916
  6.5 4.1 %copy-start.20 = (bf16[512,64]{0,1:T(8,128)(2,1)S(1)}, bf16[512,64]{0,1:T(8,128)(2,1)}, u32[]{:S(2)}) copy-start(bf16[512,64]{0,1:T(8,128)(2,1)} %param.22) | copy-start | bytes 196612
  6.5 17.0 %copy-start.17 = (bf16[1,256,2048]{2,1,0:T(8,128)(2,1)S(1)}, bf16[1,256,2048]{2,1,0:T(8,128)(2,1)}, u32[]{:S(2)}) copy-start(bf16[1,256,2048]{2,1,0:T(8,128)(2,1)} %param.19) | copy-start | bytes 3145732
  6.5 68.7 %all-gather.11.cloned.1.call-start = ((), (), s32[]{:S(2)}) async-start(), calls=%async_computation.3 | async-start | bytes 1802240 | tf_op jit(solution)/shard_map/all_gather | solution.py:237
  9.5 109.0 %all-gather.9.cloned.1.call-start = ((), (), s32[]{:S(2)}) async-start(), calls=%async_computation.2 | async-start | bytes 3342336 | tf_op jit(solution)/shard_map/all_gather | solution.py:264
  10.7 13.6 %copy-start.21 = (f32[2048]{0:T(1024)S(1)}, f32[2048]{0:T(1024)}, u32[]{:S(2)}) copy-start(f32[2048]{0:T(1024)} %param.20) | copy-start | bytes 24580
  24.3 22.4 %copy-start.23 = (f32[96]{0:T(128)S(1)}, f32[96]{0:T(128)}, u32[]{:S(2)}) copy-start(f32[96]{0:T(128)} %param.30) | copy-start | bytes 1156
  47.4 3.4 %copy-start.16 = (f32[512]{0:T(512)S(1)}, f32[512]{0:T(512)}, u32[]{:S(2)}) copy-start(f32[512]{0:T(512)} %param.28) | copy-start | bytes 6148
  47.7 3.1 %copy-start.5 = (f32[256,128]{1,0:T(8,128)}, f32[256,128]{1,0:T(8,128)S(1)}, u32[]{:S(2)}) copy-start(f32[256,128]{1,0:T(8,128)S(1)} %get-tuple-element.13.down_ref) | copy-start | bytes 393220
  47.7 3.1 %copy-start.7 = (f32[256,128]{1,0:T(8,128)}, f32[256,128]{1,0:T(8,128)S(1)}, u32[]{:S(2)}) copy-start(f32[256,128]{1,0:T(8,128)S(1)} %get-tuple-element.14.up_ref) | copy-start | bytes 393220
  47.7 5.3 %copy-start.9 = (f32[256,128]{1,0:T(8,128)}, f32[256,128]{1,0:T(8,128)S(1)}, u32[]{:S(2)}) copy-start(f32[256,128]{1,0:T(8,128)S(1)} %get-tuple-element.22.cos_ref) | copy-start | bytes 393220
  49.4 3.7 %copy-start.18 = (bf16[128,512]{1,0:T(8,128)(2,1)S(1)}, bf16[128,512]{1,0:T(8,128)(2,1)}, u32[]{:S(2)}) copy-start(bf16[128,512]{1,0:T(8,128)(2,1)} %param.36) | copy-start | bytes 393220
  53.0 25.5 %copy-start.22 = (bf16[31,128]{1,0:T(8,128)(2,1)S(1)}, bf16[31,128]{1,0:T(8,128)(2,1)}, u32[]{:S(2)}) copy-start(bf16[31,128]{1,0:T(8,128)(2,1)} %param.33) | copy-start | bytes 23812
  75.2 1.4 copy-start
  76.6 18.9 %copy-start.1 = (bf16[2816,256]{1,0:T(8,128)(2,1)S(1)}, bf16[2816,256]{1,0:T(8,128)(2,1)}, u32[]{:S(2)}) copy-start(bf16[2816,256]{1,0:T(8,128)(2,1)} %all-gather.11.cloned.1.call-done) | copy-start | bytes 4325380
  77.0 41.5 %copy-start.3 = (bf16[512,512]{1,0:T(8,128)(2,1)S(1)}, bf16[512,512]{1,0:T(8,128)(2,1)}, u32[]{:S(2)}) copy-start(bf16[512,512]{1,0:T(8,128)(2,1)} %all-gather.3) | copy-start | bytes 1572868
  77.0 41.5 %copy-start.4 = (bf16[512,512]{1,0:T(8,128)(2,1)S(1)}, bf16[512,512]{1,0:T(8,128)(2,1)}, u32[]{:S(2)}) copy-start(bf16[512,512]{1,0:T(8,128)(2,1)} %all-gather.4) | copy-start | bytes 1572868
  77.1 2.2 %collective-permute-start = (bf16[32,128]{1,0:T(8,128)(2,1)S(1)}, bf16[32,128]{1,0:T(8,128)(2,1)S(1)}, u32[]{:S(2)}, u32[]{:S(2)}) collective-permute-start(bf16[32,128]{1,0:T(8,128)(2,1)S(1)} %slice.33), channel_id=1, source_target_pairs={{0,32},{32,64},{64,96},{96,128},{128,160},{160,192},{192,224},{224... | collective-permute-start | bytes 24584 | tf_op jit(solution)/shard_map/ppermute | solution.py:274
  79.7 0.7 copy-start.13
  80.4 0.7 copy-start.14
  81.0 0.7 copy-start.15
  84.4 16.9 %all-to-all-start = ((f32[8,1,512]{2,1,0:T(1,128)}), f32[8,1,512]{2,1,0:T(1,128)S(1)}, u32[]{:S(2)}, u32[]{:S(2)}) async-start(f32[8,1,512]{2,1,0:T(1,128)} %broadcast_in_dim.48), calls=%async_computation | async-start | bytes 32768 | tf_op jit(solution)/shard_map/all_to_all | solution.py:284
  95.5 0.9 copy-start.6
  96.4 0.9 copy-start.8
  97.3 0.9 copy-start.10
  100.6 0.7 copy-start.11
  118.5 1.9 %copy-start.2 = (bf16[4096,384]{1,0:T(8,128)(2,1)S(1)}, bf16[4096,384]{1,0:T(8,128)(2,1)}, u32[]{:S(2)}) copy-start(bf16[4096,384]{1,0:T(8,128)(2,1)} %all-gather.9.cloned.1.call-done.kv_ref) | copy-start | bytes 9437188
  120.4 0.9 copy-start.12
  161.7 7.8 %collective-permute-start.1 = (bf16[4,32,2048]{2,1,0:T(8,128)(2,1)S(1)}, bf16[4,32,2048]{2,1,0:T(8,128)(2,1)S(1)}, u32[]{:S(2)}, u32[]{:S(2)}) collective-permute-start(bf16[4,32,2048]{2,1,0:T(8,128)(2,1)S(1)} %bitcast.53), channel_id=1, source_target_pairs={{0,1},{1,0},{2,3},{3,2},{4,5},{5,4},{6,7},{7,6},{8,9},{9,8},{10,11... | collective-permute-start | bytes 1572872 | tf_op jit(solution)/shard_map/ppermute | solution.py:303
Sparse Core Ops, SparseCore 0:
  9.7 38.1 all-gather.10
  53.2 65.2 all-gather.8
